TPU v7x, 32 devices: a whole 2x2x4 slice. The times are simulated.
32 devices in a mesh: grp: 2 (over y), fs: 4 (over z), tp: 4 (over x, core).
Axes of the slice: x: 2, y: 2, z: 4, core: 2. Of those that a mesh axis runs over, the one named last changes fastest.
Arguments:
- tokens: bfloat16 [32, 128, 2048], P(('grp', 'fs'), None, 'tp'), parts along dimension 0, may hold values from -100 to 100
- mix_gain: float32 [2048], replicated, may hold values from 0.1 to 1.9
- gate_outer: bfloat16 [2048, 1024], P('fs', 'tp'), may hold values from -0.125 to 0.125
- gate_inner: bfloat16 [2048, 1024], P('fs', 'tp'), may hold values from -0.125 to 0.125
- value_weight: bfloat16 [2048, 1024], P('fs', 'tp'), may hold values from -0.125 to 0.125
- conv_taps: float32 [3, 1024], replicated, may hold values from -3 to 3
- mix_out: bfloat16 [1024, 2048], P('tp', 'fs'), may hold values from -0.25 to 0.25
- ffn_gain: float32 [2048], replicated, may hold values from 0.1 to 1.9
- ffn_gate: bfloat16 [2048, 5632], P('fs', 'tp'), may hold values from -0.125 to 0.125
- ffn_up: bfloat16 [2048, 5632], P('fs', 'tp'), may hold values from -0.125 to 0.125
- ffn_down: bfloat16 [5632, 2048], P('tp', 'fs'), may hold values from -0.109375 to 0.109375
- out_gain: float32 [2048], replicated, may hold values from 0.1 to 1.9
Outputs:
- layer_out: bfloat16 [32, 128, 2048], P(('grp', 'fs'), None, 'tp'), parts along dimension 0
There are 2 independent parts, one for each index of `grp`. A program takes and returns all parts, laid end to end along the dimension named above; an argument that names none is the same for every part. Nothing has to cross between parts.
All inputs are finite; a program needn't handle non-finite values.
Results may differ from a plain program's by a relative error of at most 0.015.
Values may be sent and summed in bfloat16 or wider, within the bound.
A program may use at most 64 MiB of HBM per device.

v0:
```python
import jax
import jax.numpy as jnp
from jax import lax
from jax.sharding import PartitionSpec as P


def rms_norm(values, gain):
    floats = values.astype(jnp.float32)
    scaled = floats * lax.rsqrt(jnp.mean(floats * floats, axis=-1, keepdims=True) + 1e-06)
    return (scaled * gain).astype(jnp.bfloat16)


def local(
    tokens,
    mix_gain,
    gate_outer,
    gate_inner,
    value_weight,
    conv_taps,
    mix_out,
    ffn_gain,
    ffn_gate,
    ffn_up,
    ffn_down,
    out_gain,
):
    seq_count, length, columns = tokens.shape
    row_count = seq_count * length
    width = columns * lax.axis_size("tp")
    whole = lax.all_gather(tokens, "tp", axis=2, tiled=True).reshape(row_count, width)
    normed = rms_norm(whole, mix_gain)
    channels = gate_outer.shape[1]
    pieces = (
        lax.all_gather(gate_outer, "fs", axis=0, tiled=True),
        lax.all_gather(gate_inner, "fs", axis=0, tiled=True),
        lax.all_gather(value_weight, "fs", axis=0, tiled=True),
    )
    sliced = normed
    outer = jnp.dot(sliced, pieces[0], preferred_element_type=jnp.float32)
    inner = jnp.dot(sliced, pieces[1], preferred_element_type=jnp.float32)
    values = jnp.dot(sliced, pieces[2], preferred_element_type=jnp.float32)
    outer = outer.astype(jnp.bfloat16)
    inner = inner.astype(jnp.bfloat16)
    values = values.astype(jnp.bfloat16)
    product = (inner.astype(jnp.float32) * values.astype(jnp.float32)).reshape(
        seq_count, length, channels
    )
    own_taps = lax.dynamic_slice_in_dim(conv_taps, lax.axis_index("tp") * channels, channels, 1)
    tap_count = conv_taps.shape[0]
    padded = jnp.pad(product, ((0, 0), (tap_count - 1, 0), (0, 0)))
    conv = jnp.zeros((seq_count, length, channels), jnp.float32)
    for offset in range(tap_count):
        conv = conv + own_taps[offset] * padded[:, offset : offset + length]
    gated = (outer.astype(jnp.float32) * conv.reshape(row_count, channels)).astype(jnp.bfloat16)
    mix_terms = jnp.dot(
        gated, lax.all_gather(mix_out, "fs", axis=1, tiled=True), preferred_element_type=jnp.float32
    )
    mix_full = lax.psum(mix_terms.astype(jnp.bfloat16), "tp").astype(jnp.float32)
    first_full = (whole.astype(jnp.float32) + mix_full).astype(jnp.bfloat16)
    first = lax.dynamic_slice_in_dim(first_full, lax.axis_index("tp") * columns, columns, 1)
    normed_ffn = rms_norm(first_full, ffn_gain)
    pieces = (
        lax.all_gather(ffn_gate, "fs", axis=0, tiled=True),
        lax.all_gather(ffn_up, "fs", axis=0, tiled=True),
    )
    sliced = normed_ffn
    gate = jnp.dot(sliced, pieces[0], preferred_element_type=jnp.float32)
    upward = jnp.dot(sliced, pieces[1], preferred_element_type=jnp.float32)
    hidden = (jax.nn.silu(gate) * upward).astype(jnp.bfloat16)
    down_terms = jnp.dot(
        hidden,
        lax.all_gather(ffn_down, "fs", axis=1, tiled=True),
        preferred_element_type=jnp.float32,
    )
    down_summed = lax.psum_scatter(
        down_terms.astype(jnp.bfloat16), "tp", scatter_dimension=1, tiled=True
    ).astype(jnp.float32)
    second = first.astype(jnp.float32) + down_summed
    squares = lax.psum(jnp.sum(second * second, axis=1), "tp")
    factor = lax.rsqrt(squares / width + 1e-06)
    own_gain = lax.dynamic_slice_in_dim(out_gain, lax.axis_index("tp") * columns, columns, 0)
    result = second * factor[:, None] * own_gain
    return result.astype(jnp.bfloat16).reshape(seq_count, length, columns)


def solution(mesh):
    in_specs = (
        P(("grp", "fs"), None, "tp"),
        P(),
        P("fs", "tp"),
        P("fs", "tp"),
        P("fs", "tp"),
        P(),
        P("tp", "fs"),
        P(),
        P("fs", "tp"),
        P("fs", "tp"),
        P("tp", "fs"),
        P(),
    )
    out_specs = P(("grp", "fs"), None, "tp")
    return jax.shard_map(local, mesh=mesh, in_specs=in_specs, out_specs=out_specs, check_vma=False)
```

profile of v0, /device:TPU:16, one launch (start us, length us, event | category | flops | bytes accessed | tf_op | source)
XLA Modules:
  0.0 585.5 jit_solution(15794149463791373341)
XLA Ops:
  6.5 0.7 all-gather.9.cloned.1.call-update
  7.3 0.7 all-gather.15.cloned.1.call-update
  10.0 0.9 constant_dynamic-slice_fusion
  10.8 21.7 %all-gather.9.cloned.1.call-done = bf16[4,128,2048]{2,1,0:T(8,128)(2,1)} async-done(((bf16[4,128,512]{2,1,0:T(8,128)(2,1)}), bf16[4,128,2048]{2,1,0:T(8,128)(2,1)}) %all-gather.9.cloned.1.call-update) | async-done | bytes 2097168 | tf_op jit(solution)/shard_map/all_gather | solution.py:30
  32.6 2.2 fusion.3
  35.4 26.2 %all-gather.15.cloned.1.call-done = bf16[2048,256]{1,0:T(8,128)(2,1)} async-done(((bf16[512,256]{1,0:T(8,128)(2,1)}), bf16[2048,256]{1,0:T(8,128)(2,1)}) %all-gather.15.cloned.1.call-update) | async-done | bytes 1048592 | tf_op jit(solution)/shard_map/all_gather | solution.py:36
  61.5 1.9 fusion.13
  63.5 27.0 %all-gather.13.cloned.1.call-done = bf16[2048,256]{1,0:T(8,128)(2,1)} async-done(((bf16[512,256]{1,0:T(8,128)(2,1)}), bf16[2048,256]{1,0:T(8,128)(2,1)}) %all-gather.13.cloned.1.call-update) | async-done | bytes 1048592 | tf_op jit(solution)/shard_map/all_gather | solution.py:35
  90.5 1.9 fusion.12
  92.6 26.7 %all-gather.11.cloned.1.call-done = bf16[2048,256]{1,0:T(8,128)(2,1)} async-done(((bf16[512,256]{1,0:T(8,128)(2,1)}), bf16[2048,256]{1,0:T(8,128)(2,1)}) %all-gather.11.cloned.1.call-update) | async-done | bytes 1048592 | tf_op jit(solution)/shard_map/all_gather | solution.py:34
  119.3 28.8 %all-gather.17.cloned.1.call-done = bf16[256,2048]{1,0:T(8,128)(2,1)} async-done(((bf16[256,512]{1,0:T(8,128)(2,1)}), bf16[256,2048]{1,0:T(8,128)(2,1)}) %all-gather.17.cloned.1.call-update) | async-done | bytes 1048592 | tf_op jit(solution)/shard_map/all_gather | solution.py:56
  148.1 5.2 convolution_convert_fusion
  155.8 49.0 %all-reduce.3.cloned.1.call-done = bf16[512,2048]{1,0:T(8,128)(2,1)} async-done(((bf16[512,2048]{1,0:T(8,128)(2,1)}), bf16[512,2048]{1,0:T(8,128)(2,1)}) %all-reduce.3.cloned.1.call-update) | async-done | bytes 2097168 | tf_op jit(solution)/shard_map/psum | solution.py:58
  204.9 3.9 fusion
  208.8 102.7 %all-gather.19.cloned.1.call-done = bf16[2048,1408]{1,0:T(8,128)(2,1)} async-done(((bf16[512,1408]{1,0:T(8,128)(2,1)}), bf16[2048,1408]{1,0:T(8,128)(2,1)}) %all-gather.19.cloned.1.call-update) | async-done | bytes 5767184 | tf_op jit(solution)/shard_map/all_gather | solution.py:63
  311.5 8.4 %fusion.16 = f32[512,1408]{1,0:T(8,128)} fusion(bf16[2048,1408]{1,0:T(8,128)(2,1)} %all-gather.19.cloned.1.call-done, bf16[512,2048]{1,0:T(8,128)(2,1)} %get-tuple-element.6, f32[2048]{0:T(1024)S(1)} %copy-done.4, f32[512]{0:T(512)S(1)} %add_rsqrt_fusion.1), kind=kOutput, calls=%fused_computation.28 | convolution fusion | flops 2956984320 | bytes 10758144 | tf_op jit(solution)/shard_map/dot_general | solution.py:67
  319.9 98.1 %all-gather.21.cloned.1.call-done = bf16[2048,1408]{1,0:T(8,128)(2,1)} async-done(((bf16[512,1408]{1,0:T(8,128)(2,1)}), bf16[2048,1408]{1,0:T(8,128)(2,1)}) %all-gather.21.cloned.1.call-update) | async-done | bytes 5767184 | tf_op jit(solution)/shard_map/all_gather | solution.py:64
  418.1 106.5 %all-gather.23.cloned.1.call-done = bf16[1408,2048]{1,0:T(8,128)(2,1)} async-done(((bf16[1408,512]{1,0:T(8,128)(2,1)}), bf16[1408,2048]{1,0:T(8,128)(2,1)}) %all-gather.23.cloned.1.call-update) | async-done | bytes 5767184 | tf_op jit(solution)/shard_map/all_gather | solution.py:72
  524.6 13.4 %convolution_convert_fusion.1 = bf16[512,2048]{1,0:T(8,128)(2,1)} fusion(bf16[1408,2048]{1,0:T(8,128)(2,1)} %all-gather.23.cloned.1.call-done, bf16[2048,1408]{1,0:T(8,128)(2,1)} %all-gather.21.cloned.1.call-done, f32[512,1408]{1,0:T(8,128)} %fusion.16, bf16[512,2048]{1,0:T(8,128)(2,1)S(1)} %copy-done.2, f32[2048]{0:T(1024)S(1)} %copy-done.4, ...), kind=kOutput, calls=%fused_computation.15 | convolution fusion | flops 5915148288 | bytes 18622464 | tf_op jit(solution)/shard_map/dot_general | solution.py:70
  538.1 0.8 dynamic_slice.11
  538.8 30.5 %reduce-scatter.2.cloned.1.call-done = bf16[512,512]{1,0:T(8,128)(2,1)} async-done(((bf16[512,2048]{1,0:T(8,128)(2,1)}), bf16[512,512]{1,0:T(8,128)(2,1)}) %reduce-scatter.2.cloned.1.call-update) | async-done | bytes 524304 | tf_op jit(solution)/shard_map/reduce_scatter | solution.py:75
  569.4 1.3 multiply_reduce_fusion
  570.6 6.0 %psum.15 = f32[512]{0:T(512)S(1)} all-reduce(f32[512]{0:T(512)S(1)} %multiply_reduce_fusion), channel_id=1, replica_groups=mesh['grp'=2,'fs'=4,'tp'=4] {'tp'}, use_global_device_ids=true, to_apply=%region_5.6 | all-reduce | flops 512 | bytes 4096 | tf_op jit(solution)/shard_map/psum | solution.py:79
  576.6 2.0 multiply_convert_fusion
  (33 shorter events, 5.1 us)
Async XLA Ops:
  6.5 28.3 %copy-start.3 = (f32[2048]{0:T(1024)S(1)}, f32[2048]{0:T(1024)}, u32[]{:S(2)}) copy-start(f32[2048]{0:T(1024)} %param.13) | copy-start | bytes 24580
  6.5 26.0 %all-gather.9.cloned.1.call-start = ((), (), s32[]{:S(2)}) async-start(), calls=%async_computation.1 | async-start | bytes 2621440 | tf_op jit(solution)/shard_map/all_gather | solution.py:30
  7.3 54.3 %all-gather.15.cloned.1.call-start = ((), (), s32[]{:S(2)}) async-start(), calls=%async_computation.4 | async-start | bytes 1310720 | tf_op jit(solution)/shard_map/all_gather | solution.py:36
  8.0 82.5 %all-gather.13.cloned.1.call-start = ((), (), s32[]{:S(2)}) async-start(), calls=%async_computation.3 | async-start | bytes 1310720 | tf_op jit(solution)/shard_map/all_gather | solution.py:35
  8.7 110.6 %all-gather.11.cloned.1.call-start = ((), (), s32[]{:S(2)}) async-start(), calls=%async_computation.2 | async-start | bytes 1310720 | tf_op jit(solution)/shard_map/all_gather | solution.py:34
  9.3 138.8 %all-gather.17.cloned.1.call-start = ((), (), s32[]{:S(2)}) async-start(), calls=%async_computation.5 | async-start | bytes 1310720 | tf_op jit(solution)/shard_map/all_gather | solution.py:56
  9.9 195.0 %all-reduce.3.cloned.1.call-start = ((), (), s32[]{:S(2)}) async-start(), calls=%async_computation.6 | async-start | bytes 4194304 | tf_op jit(solution)/shard_map/psum | solution.py:58
  32.6 2.2 copy-start
  153.3 51.5 %copy-start.1 = (bf16[4,128,2048]{2,1,0:T(8,128)(2,1)S(1)}, bf16[4,128,2048]{2,1,0:T(8,128)(2,1)}, u32[]{:S(2)}) copy-start(bf16[4,128,2048]{2,1,0:T(8,128)(2,1)} %all-gather.9.cloned.1.call-done) | copy-start | bytes 6291460
  153.4 158.2 %all-gather.19.cloned.1.call-start = ((), (), s32[]{:S(2)}) async-start(), calls=%async_computation.7 | async-start | bytes 7208960 | tf_op jit(solution)/shard_map/all_gather | solution.py:63
  154.1 263.9 %all-gather.21.cloned.1.call-start = ((), (), s32[]{:S(2)}) async-start(), calls=%async_computation.8 | async-start | bytes 7208960 | tf_op jit(solution)/shard_map/all_gather | solution.py:64
  154.9 369.7 %all-gather.23.cloned.1.call-start = ((), (), s32[]{:S(2)}) async-start(), calls=%async_computation.9 | async-start | bytes 7208960 | tf_op jit(solution)/shard_map/all_gather | solution.py:72
  155.6 155.9 %copy-start.4 = (f32[2048]{0:T(1024)S(1)}, f32[2048]{0:T(1024)}, u32[]{:S(2)}) copy-start(f32[2048]{0:T(1024)} %param.19) | copy-start | bytes 24580
  155.6 413.7 %reduce-scatter.2.cloned.1.call-start = ((), (), s32[]{:S(2)}) async-start(), calls=%async_computation.10 | async-start | bytes 2621440 | tf_op jit(solution)/shard_map/reduce_scatter | solution.py:75
  311.5 213.1 %copy-start.2 = (bf16[512,2048]{1,0:T(8,128)(2,1)S(1)}, bf16[512,2048]{1,0:T(8,128)(2,1)}, u32[]{:S(2)}) copy-start(bf16[512,2048]{1,0:T(8,128)(2,1)} %get-tuple-element.6) | copy-start | bytes 6291460
Sparse Core Ops, SparseCore 0:
  8.9 23.6 all-gather.8
  34.1 27.3 all-gather.14
  63.1 27.3 all-gather.12
  91.9 27.3 all-gather.10
  120.7 27.3 all-gather.16
  153.5 51.3 all-reduce.2
  206.4 105.0 all-gather.18
  313.1 104.9 all-gather.20
  419.6 104.9 all-gather.22
  538.2 31.1 reduce-scatter.1
where the time goes:
time: 587 us; the launch traced here: 586 us
  waiting for transfers between devices  523 us (89%)
  matrix products  30.9 us (5%)
  between operations  13.6 us (2%)
  other arithmetic  10.2 us (2%)
  blocking collectives  5.97 us (1%)
    all_gather x1, waiting for transfers between devices, local(): lax.all_gather(ffn_down, 'fs', axis=1, tiled=True)  107 us
    all_gather x1, waiting for transfers between devices, local(): lax.all_gather(ffn_gate, 'fs', axis=0, tiled=True)  103 us
    all_gather x1, waiting for transfers between devices, local(): lax.all_gather(ffn_up, 'fs', axis=0, tiled=True)  98.1 us
    psum x1, waiting for transfers between devices, local(): lax.psum(mix_terms.astype(jnp.bfloat16), 'tp').astype(jnp.float32)  49 us
    reduce_scatter x1, waiting for transfers between devices, local(): lax.psum_scatter(down_terms.astype(jnp.bfloat16), 'tp', scatter_dimension...  30.5 us
    all_gather x1, waiting for transfers between devices, local(): lax.all_gather(mix_out, 'fs', axis=1, tiled=True)  28.8 us
    all_gather x1, waiting for transfers between devices, local(): lax.all_gather(gate_inner, 'fs', axis=0, tiled=True)  27 us
    all_gather x1, waiting for transfers between devices, local(): lax.all_gather(gate_outer, 'fs', axis=0, tiled=True)  26.7 us
  transfers between devices with their start and end apart: 10, of which 10 were waited for; matrix products, arithmetic and copies ran while one was open for 4% of the time, Pallas kernels for 0%

commit v1 on v0

v1 whole, which is shorter than its diff:
```python
import functools

import jax
import jax.numpy as jnp
from jax import lax
from jax.experimental import pallas as pl
from jax.experimental.pallas import tpu as pltpu
from jax.sharding import PartitionSpec as P

MESH = pl.DeviceIdType.MESH
F32 = jnp.float32
BF16 = jnp.bfloat16
MIXER = 4
GATE, UP, DOWN = 4, 5, 6


def chunks_of(half):
    return next(count for count in (4, 2, 1) if half % (count * 16) == 0 or count == 1)


def column(rows):
    wide = jnp.broadcast_to(rows, (rows.shape[1], rows.shape[1]))
    return jnp.transpose(wide)[:, :1]


def kernel(
    n, parts, n_tp, length, chunk_counts,
    tok_ref, mix_gain, w0, w1, w2, taps_ref, w3, ffn_gain, w4, w5, w6, out_gain,
    out_ref,
    f0, f1, f2, f3, f4, f5, f6,
    tok_full, normed, proj, gated, mix_part, mix_recv, first_full, hidden, down_part, down_recv, sq_send, sq_recv,
    right_send, left_send, z_recv, y_send, y_recv, own_sem, tp_send, tp_recv, down_send, down_rsem,
):
    own = (w0, w1, w2, w3, w4, w5, w6)
    full = (f0, f1, f2, f3, f4, f5, f6)
    f, g, t = lax.axis_index("fs"), lax.axis_index("grp"), lax.axis_index("tp")
    rows, columns = tok_ref.shape
    width = columns * n_tp
    seqs = rows // length
    bases = [sum(chunk_counts[:w]) for w in range(7)]

    def y_peer(k):
        return lax.rem(g + k, parts)

    def tp_peer(k):
        return lax.rem(t + k, n_tp)

    def span(w, half, c):
        size = own[w].shape[0] // parts
        piece = size // chunk_counts[w]
        start = half * size + c * piece
        return pl.ds(pl.multiple_of(start, 8), piece)

    def region(w, blk, half, c):
        return full[w].at[blk, span(w, half, c), :]

    barrier = pltpu.get_barrier_semaphore()
    for k in range(1, n_tp):
        pl.semaphore_signal(barrier, inc=1, device_id={"tp": tp_peer(k)}, device_id_type=MESH)
    for k in range(1, parts):
        pl.semaphore_signal(barrier, inc=1, device_id={"grp": y_peer(k)}, device_id_type=MESH)

    @pl.when(f < n - 1)
    def _():
        pl.semaphore_signal(barrier, inc=1, device_id={"fs": f + 1}, device_id_type=MESH)

    @pl.when(f > 0)
    def _():
        pl.semaphore_signal(barrier, inc=1, device_id={"fs": f - 1}, device_id_type=MESH)

    neighbours = lax.min(f, 1) + lax.min(n - 1 - f, 1)
    pl.semaphore_wait(barrier, n_tp - 1 + parts - 1 + neighbours)

    def z_copy(w, c, blk, src, step):
        send = right_send if step > 0 else left_send
        return pltpu.make_async_remote_copy(
            src_ref=src, dst_ref=region(w, blk, g, c),
            send_sem=send.at[bases[w] + c, blk], recv_sem=z_recv.at[bases[w] + c, blk],
            device_id={"fs": f + step}, device_id_type=MESH,
        )

    def y_copy(w, c, blk, half, k, peer):
        return pltpu.make_async_remote_copy(
            src_ref=region(w, blk, half, c), dst_ref=region(w, blk, half, c),
            send_sem=y_send.at[bases[w] + c, blk, k - 1], recv_sem=y_recv.at[bases[w] + c, blk, k - 1],
            device_id={"grp": peer}, device_id_type=MESH,
        )

    def start_own(w):
        @pl.loop(0, chunk_counts[w])
        def _(c):
            src = own[w].at[span(w, g, c), :]

            @pl.when(f < n - 1)
            def _():
                z_copy(w, c, f, src, 1).start()

            @pl.when(f > 0)
            def _():
                z_copy(w, c, f, src, -1).start()

    def receive(w, s):
        left, right = f - 1 - s, f + 1 + s

        @pl.loop(0, chunk_counts[w])
        def _(c):
            def arrived(blk, step):
                z_copy(w, c, blk, region(w, blk, g, c), -step).wait_recv()
                onward = (f < n - 1) if step > 0 else (f > 0)

                @pl.when(onward)
                def _():
                    z_copy(w, c, blk, region(w, blk, g, c), step).start()

                for k in range(1, parts):
                    y_copy(w, c, blk, g, k, y_peer(k)).start()

            @pl.when(left >= 0)
            def _():
                arrived(left, 1)

            @pl.when(right < n)
            def _():
                arrived(right, -1)

    def finish(w, s):
        @pl.loop(0, chunk_counts[w])
        def _(c):
            for k in range(1, parts):
                source = lax.rem(g + parts - k, parts)
                for blk, there in ((f - 1 - s, f - 1 - s >= 0), (f + 1 + s, f + 1 + s < n)):
                    @pl.when(there)
                    def _():
                        y_copy(w, c, blk, source, k, source).wait_recv()

    def own_copy(w):
        return pltpu.make_async_copy(own[w], full[w].at[f], own_sem.at[w])

    def tp_copy(stage, k, src, dst, peer):
        return pltpu.make_async_remote_copy(
            src_ref=src, dst_ref=dst, send_sem=tp_send.at[stage, k - 1], recv_sem=tp_recv.at[stage, k - 1],
            device_id={"tp": peer}, device_id_type=MESH,
        )

    def own_columns(owner):
        return pl.ds(pl.multiple_of(owner * columns, 128), columns)

    def source_of(k):
        return lax.rem(t + n_tp - k, n_tp)

    for w in range(MIXER):
        start_own(w)
    for k in range(1, n_tp):
        tp_copy(0, k, tok_ref, tok_full.at[:, own_columns(t)], tp_peer(k)).start()
    for w in range(7):
        own_copy(w).start()
    own_tokens = pltpu.make_async_copy(tok_ref, tok_full.at[:, own_columns(t)], own_sem.at[7])
    own_tokens.start()
    for w in range(MIXER):
        for s in range(n - 1):
            receive(w, s)
        if w == 2:
            start_own(GATE)

    def norm_rows(source, gain):
        size = 32

        @pl.loop(0, rows // size)
        def _(i):
            at = pl.ds(pl.multiple_of(i * size, size), size)
            values = source[at, :].astype(F32)
            scale = lax.rsqrt(jnp.sum(values * values, axis=1, keepdims=True) / width + 1e-06)
            normed[at, :] = (values * scale * gain[...]).astype(BF16)

    own_tokens.wait()
    for k in range(1, n_tp):
        tp_copy(0, k, tok_ref, tok_full.at[:, own_columns(source_of(k))], tp_peer(k)).wait_recv()
    norm_rows(tok_full, mix_gain)
    channels = w0.shape[1]
    for w in range(MIXER):
        own_copy(w).wait()
        for s in range(n - 1):
            finish(w, s)
    for w in range(3):
        weight = full[w][...].reshape(width, channels)
        proj[w] = jnp.dot(normed[...], weight, preferred_element_type=F32).astype(BF16)
    taps = taps_ref[:, pl.ds(pl.multiple_of(t * channels, 128), channels)]
    tap_count = taps_ref.shape[0]

    @pl.loop(0, seqs)
    def _(i):
        at = pl.ds(pl.multiple_of(i * length, length), length)
        product = proj[1, at, :].astype(F32) * proj[2, at, :].astype(F32)
        position = lax.broadcasted_iota(jnp.int32, product.shape, 0)
        conv = jnp.zeros_like(product)
        for offset in range(tap_count):
            shift = tap_count - 1 - offset
            moved = product if shift == 0 else jnp.where(position >= shift, pltpu.roll(product, shift, 0), 0.0)
            conv = conv + taps[offset : offset + 1, :] * moved
        gated[at, :] = (proj[0, at, :].astype(F32) * conv).astype(BF16)

    block = w3.shape[1]

    @pl.loop(0, n)
    def _(b):
        at = pl.ds(pl.multiple_of(b * block, 128), block)
        mix_part[:, at] = jnp.dot(gated[...], full[3][b], preferred_element_type=F32).astype(BF16)

    for k in range(1, n_tp):
        peer = tp_peer(k)
        tp_copy(1, k, mix_part.at[:, own_columns(peer)], mix_recv.at[k - 1], peer).start()

    for s in range(n - 1):
        if s == n - 2:
            start_own(UP)
        receive(GATE, s)

    for k in range(1, n_tp):
        tp_copy(1, k, mix_part.at[:, own_columns(t)], mix_recv.at[k - 1], source_of(k)).wait_recv()

    @pl.loop(0, rows // 64)
    def _(i):
        at = pl.ds(pl.multiple_of(i * 64, 64), 64)
        total = mix_part[at, own_columns(t)].astype(F32)
        for k in range(1, n_tp):
            total = total + mix_recv[k - 1, at, :].astype(F32)
        first_full[at, own_columns(t)] = (tok_ref[at, :].astype(F32) + total).astype(BF16)

    for k in range(1, n_tp):
        mine = first_full.at[:, own_columns(t)]
        tp_copy(2, k, mine, mine, tp_peer(k)).start()

    for s in range(n - 1):
        if s == n - 2:
            start_own(DOWN)
        receive(UP, s)

    for k in range(1, n_tp):
        theirs = first_full.at[:, own_columns(source_of(k))]
        tp_copy(2, k, theirs, theirs, source_of(k)).wait_recv()
    norm_rows(first_full, ffn_gain)
    for w in (GATE, UP):
        own_copy(w).wait()
        for s in range(n - 1):
            finish(w, s)

    units = w4.shape[1]

    def hidden_tile(start, size):
        at = pl.ds(start, size)
        gate = jnp.dot(normed[...], full[GATE][:, :, at].reshape(width, size), preferred_element_type=F32)
        upward = jnp.dot(normed[...], full[UP][:, :, at].reshape(width, size), preferred_element_type=F32)
        hidden[:, at] = (gate / (1.0 + jnp.exp(-gate)) * upward).astype(BF16)

    @pl.loop(0, units // 256)
    def _(j):
        hidden_tile(pl.multiple_of(j * 256, 256), 256)

    if units % 256:
        hidden_tile(units // 256 * 256, units % 256)

    wide = w6.shape[1]
    piece = min(wide, columns)
    per_block, per_owner = wide // piece, columns // piece

    def down_copy(sender, owner, slot, start):
        k = lax.rem(owner - sender + n_tp, n_tp)
        inside = pl.ds(pl.multiple_of(slot * piece, 128), piece)
        return pltpu.make_async_remote_copy(
            src_ref=down_part.at[:, pl.ds(start, piece)], dst_ref=down_recv.at[k, :, inside],
            send_sem=down_send.at[k, slot], recv_sem=down_rsem.at[k, slot],
            device_id={"tp": owner}, device_id_type=MESH,
        )

    def down_block(b):
        for p in range(per_block):
            start = pl.multiple_of(b * wide + p * piece, 128)
            owner = (b * wide + p * piece) // columns
            slot = lax.rem(b * per_block + p, per_owner)
            weight = full[DOWN][b][:, p * piece : (p + 1) * piece]
            down_part[:, pl.ds(start, piece)] = jnp.dot(
                hidden[...], weight, preferred_element_type=F32
            ).astype(BF16)

            @pl.when(owner != t)
            def _():
                down_copy(t, owner, slot, start).start()

    own_copy(DOWN).wait()
    down_block(f)

    @pl.loop(0, n - 1)
    def _(s):
        receive(DOWN, s)
        finish(DOWN, s)

        @pl.loop(0, 2)
        def _(side):
            b = lax.select(side == 0, f - 1 - s, f + 1 + s)

            @pl.when((b >= 0) & (b < n))
            def _():
                down_block(b)

    for k in range(1, n_tp):
        for slot in range(per_owner):
            down_copy(source_of(k), t, slot, 0).wait_recv()

    def second_rows(i):
        at = pl.ds(pl.multiple_of(i * length, length), length)
        total = down_part[at, own_columns(t)].astype(F32)
        for k in range(1, n_tp):
            total = total + down_recv[k, at, :].astype(F32)
        return at, first_full[at, own_columns(t)].astype(F32) + total

    @pl.loop(0, seqs)
    def _(i):
        _, second = second_rows(i)
        squares = jnp.sum(second * second, axis=1, keepdims=True)
        wide_squares = jnp.transpose(jnp.broadcast_to(squares, (length, length)))
        sq_send[i] = wide_squares[:8, :]

    for k in range(1, n_tp):
        tp_copy(3, k, sq_send, sq_recv.at[k - 1], tp_peer(k)).start()
    for k in range(1, n_tp):
        tp_copy(3, k, sq_send, sq_recv.at[k - 1], source_of(k)).wait_recv()

    gain = out_gain[:, own_columns(t)]

    @pl.loop(0, seqs)
    def _(i):
        at, second = second_rows(i)
        squares = sq_send[i]
        for k in range(1, n_tp):
            squares = squares + sq_recv[k - 1, i]
        factor = column(lax.rsqrt(squares[:1, :] / width + 1e-06))
        out_ref[at, :] = (second * factor * gain).astype(BF16)

    for k in range(1, n_tp):
        tp_copy(0, k, tok_ref, tok_full.at[:, own_columns(t)], tp_peer(k)).wait_send()
        tp_copy(1, k, mix_part.at[:, own_columns(t)], mix_recv.at[k - 1], tp_peer(k)).wait_send()
        tp_copy(2, k, first_full.at[:, own_columns(t)], first_full.at[:, own_columns(t)], tp_peer(k)).wait_send()
        tp_copy(3, k, sq_send, sq_recv.at[k - 1], tp_peer(k)).wait_send()
        for slot in range(per_owner):
            down_copy(t, tp_peer(k), slot, 0).wait_send()
    for w in range(7):
        @pl.loop(0, chunk_counts[w])
        def _(c):
            @pl.loop(0, n)
            def _(blk):
                here = region(w, blk, g, c)

                @pl.when((f < n - 1) & (blk <= f))
                def _():
                    z_copy(w, c, blk, here, 1).wait_send()

                @pl.when((f > 0) & (blk >= f))
                def _():
                    z_copy(w, c, blk, here, -1).wait_send()

                @pl.when(blk != f)
                def _():
                    for k in range(1, parts):
                        y_copy(w, c, blk, g, k, y_peer(k)).wait_send()


def solution(mesh):
    n, parts, n_tp = mesh.shape["fs"], mesh.shape["grp"], mesh.shape["tp"]

    def local(tokens, mix_gain, outer, inner, value, taps, mix_out, ffn_gain, gate, up, down, out_gain):
        seqs, length, columns = tokens.shape
        rows, width = seqs * length, columns * n_tp
        weights = (outer, inner, value, mix_out, gate, up, down)
        counts = tuple(1 if w < MIXER else chunks_of(a.shape[0] // parts) for w, a in enumerate(weights))
        slots = sum(counts)
        channels, units = outer.shape[1], gate.shape[1]
        others, y_others = max(n_tp - 1, 1), max(parts - 1, 1)
        per_owner = columns // min(down.shape[1], columns)
        dma = pltpu.SemaphoreType.DMA
        scratch = [pltpu.VMEM((n,) + a.shape, BF16) for a in weights]
        scratch += [
            pltpu.VMEM((rows, width), BF16),
            pltpu.VMEM((rows, width), BF16),
            pltpu.VMEM((3, rows, channels), BF16),
            pltpu.VMEM((rows, channels), BF16),
            pltpu.VMEM((rows, width), BF16),
            pltpu.VMEM((others, rows, columns), BF16),
            pltpu.VMEM((rows, width), BF16),
            pltpu.VMEM((rows, units), BF16),
            pltpu.VMEM((rows, width), BF16),
            pltpu.VMEM((n_tp, rows, columns), BF16),
            pltpu.VMEM((seqs, 8, length), F32),
            pltpu.VMEM((others, seqs, 8, length), F32),
            dma((slots, n)), dma((slots, n)), dma((slots, n)),
            dma((slots, n, y_others)), dma((slots, n, y_others)),
            dma((8,)), dma((4, others)), dma((4, others)),
            dma((n_tp, per_owner)), dma((n_tp, per_owner)),
        ]
        out = pl.pallas_call(
            functools.partial(kernel, n, parts, n_tp, length, counts),
            out_shape=jax.ShapeDtypeStruct((rows, columns), BF16),
            in_specs=[pl.BlockSpec(memory_space=pltpu.VMEM)] * 12,
            out_specs=pl.BlockSpec(memory_space=pltpu.VMEM),
            scratch_shapes=scratch,
            compiler_params=pltpu.CompilerParams(
                collective_id=0, has_side_effects=True, vmem_limit_bytes=60 * 1024 * 1024
            ),
        )(
            tokens.reshape(rows, columns), mix_gain[None], outer, inner, value, taps, mix_out,
            ffn_gain[None], gate, up, down, out_gain[None],
        )
        return out.reshape(seqs, length, columns)

    in_specs = (
        P(("grp", "fs"), None, "tp"), P(), P("fs", "tp"), P("fs", "tp"), P("fs", "tp"), P(), P("tp", "fs"),
        P(), P("fs", "tp"), P("fs", "tp"), P("tp", "fs"), P(),
    )
    out_specs = P(("grp", "fs"), None, "tp")
    return jax.shard_map(local, mesh=mesh, in_specs=in_specs, out_specs=out_specs, check_vma=False)
```

time: 587 us -> 237 us (0.40)
  the two profiles are of different devices: /device:TPU:16 before, /device:TPU:0 now
where the time goes in v1:
time: 237 us
  Pallas kernels  235 us (99%)
    pallas_call x1, Pallas kernels, local(): pl.pallas_call(functools.partial(kernel, n, parts, n_tp, length, counts),...  235 us

profile of v1, /device:TPU:0, one launch (start us, length us, event | category | flops | bytes accessed | tf_op | source)
XLA Modules:
  0.0 236.7 jit_solution(7744510566436102536)
XLA Ops:
  0.0 234.8 %shard_map.118 = bf16[512,512]{1,0:T(8,128)(2,1)} custom-call(bf16[512,512]{1,0:T(8,128)(2,1)} %bitcast.6, f32[1,2048]{1,0:T(1,128)} %bitcast.7, bf16[512,256]{1,0:T(8,128)(2,1)} %w0.1, bf16[512,256]{1,0:T(8,128)(2,1)} %w1.1, bf16[512,256]{1,0:T(8,128)(2,1)} %w2.1, f32[3,1024]{1,0:T(4,128)} %taps_ref.1, bf16[256,512]{1,0:T(8,128)(2,1)} %w3.1, ...), custom_call_target="tpu_custom_call" | custom-call | tf_op jit(solution)/shard_map/pallas_call | solution.py:399
  234.9 1.9 copy.14

commit v2 on v1

v2 whole, which is shorter than its diff:
```python
import functools

import jax
import jax.numpy as jnp
from jax import lax
from jax.experimental import pallas as pl
from jax.experimental.pallas import tpu as pltpu
from jax.sharding import PartitionSpec as P

MESH = pl.DeviceIdType.MESH
F32 = jnp.float32
BF16 = jnp.bfloat16
MIXER = 4
GATE, UP, DOWN = 4, 5, 6


def chunks_of(half):
    return next(count for count in (4, 2, 1) if half % (count * 16) == 0 or count == 1)


def column(rows):
    wide = jnp.broadcast_to(rows, (rows.shape[1], rows.shape[1]))
    return jnp.transpose(wide)[:, :1]


def kernel(
    n, parts, n_tp, length, chunk_counts,
    tok_ref, mix_gain, w0, w1, w2, taps_ref, w3, ffn_gain, w4, w5, w6, out_gain,
    out_ref,
    f0, f1, f2, f3, f4, f5, f6,
    tok_full, normed, proj, gated, part, pair_recv, far_recv, first_full, hidden, returned, sq_send, sq_recv,
    right_send, left_send, z_recv, y_send, y_recv, own_sem, pair_ss, pair_rs, far_ss, far_rs,
    down_pair_ss, down_pair_rs, down_far_ss, down_far_rs, sq_ss, sq_rs, guest_sem,
):
    own = (w0, w1, w2, w3, w4, w5, w6)
    full = (f0, f1, f2, f3, f4, f5, f6)
    f, g, t = lax.axis_index("fs"), lax.axis_index("grp"), lax.axis_index("tp")
    rows, columns = tok_ref.shape
    width = columns * n_tp
    seqs = rows // length
    bases = [sum(chunk_counts[:w]) for w in range(7)]

    def y_peer(k):
        return lax.rem(g + k, parts)

    def tp_peer(k):
        return lax.rem(t + k, n_tp)

    def span(w, half, c):
        size = own[w].shape[0] // parts
        piece = size // chunk_counts[w]
        start = half * size + c * piece
        return pl.ds(pl.multiple_of(start, 8), piece)

    def region(w, blk, half, c):
        return full[w].at[blk, span(w, half, c), :]

    barrier = pltpu.get_barrier_semaphore()
    for k in range(1, n_tp):
        pl.semaphore_signal(barrier, inc=1, device_id={"tp": tp_peer(k)}, device_id_type=MESH)
    for k in range(1, parts):
        pl.semaphore_signal(barrier, inc=1, device_id={"grp": y_peer(k)}, device_id_type=MESH)

    @pl.when(f < n - 1)
    def _():
        pl.semaphore_signal(barrier, inc=1, device_id={"fs": f + 1}, device_id_type=MESH)

    @pl.when(f > 0)
    def _():
        pl.semaphore_signal(barrier, inc=1, device_id={"fs": f - 1}, device_id_type=MESH)

    neighbours = lax.min(f, 1) + lax.min(n - 1 - f, 1)
    pl.semaphore_wait(barrier, n_tp - 1 + parts - 1 + neighbours)

    def z_copy(w, c, blk, src, step):
        send = right_send if step > 0 else left_send
        return pltpu.make_async_remote_copy(
            src_ref=src, dst_ref=region(w, blk, g, c),
            send_sem=send.at[bases[w] + c, blk], recv_sem=z_recv.at[bases[w] + c, blk],
            device_id={"fs": f + step}, device_id_type=MESH,
        )

    def y_copy(w, c, blk, half, k, peer):
        return pltpu.make_async_remote_copy(
            src_ref=region(w, blk, half, c), dst_ref=region(w, blk, half, c),
            send_sem=y_send.at[bases[w] + c, blk, k - 1], recv_sem=y_recv.at[bases[w] + c, blk, k - 1],
            device_id={"grp": peer}, device_id_type=MESH,
        )

    first_host, last_host = 1, n - 2
    is_host = (f >= first_host) & (f <= last_host)

    def start_own(w):
        @pl.loop(0, chunk_counts[w])
        def _(c):
            src = own[w].at[span(w, g, c), :]

            @pl.when(f + 1 <= last_host)
            def _():
                z_copy(w, c, f, src, 1).start()

            @pl.when(f - 1 >= first_host)
            def _():
                z_copy(w, c, f, src, -1).start()

    def other_half(w, c, k):
        half = lax.rem(g + parts - k, parts)
        inward = lax.select(f == 0, 1, n - 2)
        return pltpu.make_async_remote_copy(
            src_ref=own[w].at[span(w, half, c), :], dst_ref=region(w, f, half, c),
            send_sem=y_send.at[bases[w] + c, f, k - 1], recv_sem=y_recv.at[bases[w] + c, f, k - 1],
            device_id={"fs": inward}, device_id_type=MESH,
        )

    def receive(w, s):
        left, right = f - 1 - s, f + 1 + s

        @pl.loop(0, chunk_counts[w])
        def _(c):
            def arrived(blk, step, whole):
                z_copy(w, c, blk, region(w, blk, g, c), -step).wait_recv()
                onward = (f + 1 <= last_host) if step > 0 else (f - 1 >= first_host)

                @pl.when(onward)
                def _():
                    z_copy(w, c, blk, region(w, blk, g, c), step).start()

                def share():
                    for k in range(1, parts):
                        y_copy(w, c, blk, g, k, y_peer(k)).start()

                if s == 0:
                    pl.when(jnp.logical_not(whole))(share)
                else:
                    share()

            @pl.when(right < n)
            def _():
                arrived(right, -1, right == n - 1)

            @pl.when(left >= 0)
            def _():
                arrived(left, 1, left == 0)

    def finish(w, s):
        @pl.loop(0, chunk_counts[w])
        def _(c):
            for k in range(1, parts):
                source = lax.rem(g + parts - k, parts)
                for blk, there in ((f - 1 - s, f - 1 - s >= 0), (f + 1 + s, f + 1 + s < n)):
                    @pl.when(there)
                    def _():
                        y_copy(w, c, blk, source, k, source).wait_recv()

    def own_copy(w):
        return pltpu.make_async_copy(own[w], full[w].at[f], own_sem.at[w])

    def own_columns(owner):
        return pl.ds(pl.multiple_of(owner * columns, 128), columns)

    chips = n_tp // 2
    core = lax.rem(t, 2)
    pair = t + 1 - 2 * core

    def ahead(k, start=None):
        return lax.rem((t if start is None else start) + 2 * k, n_tp)

    def behind(k, start=None):
        return lax.rem((t if start is None else start) + n_tp - 2 * k, n_tp)

    def set_rows(r):
        return pl.ds(r * rows, rows)

    def pair_copy(stage, r, k, src, dst):
        return pltpu.make_async_remote_copy(
            src_ref=src, dst_ref=dst, send_sem=pair_ss.at[stage, r, k], recv_sem=pair_rs.at[stage, r, k],
            device_id={"tp": pair}, device_id_type=MESH,
        )

    def far_copy(stage, r, k, src, dst, peer):
        return pltpu.make_async_remote_copy(
            src_ref=src, dst_ref=dst, send_sem=far_ss.at[stage, r, k], recv_sem=far_rs.at[stage, r, k],
            device_id={"tp": peer}, device_id_type=MESH,
        )

    def block_of(buf, r, owner):
        return buf.at[set_rows(r), own_columns(owner)]

    def gather_send(buf, stage, r):
        mine = block_of(buf, r, t)
        for k in range(1, chips):
            far_copy(stage, r, k, mine, mine, ahead(k)).start()
        pair_copy(stage, r, 0, mine, mine).start()

    def gather_relay(buf, stage, r):
        for k in range(1, chips):
            theirs = block_of(buf, r, behind(k))
            far_copy(stage, r, k, theirs, theirs, behind(k)).wait_recv()
            pair_copy(stage, r, k, theirs, theirs).start()

    def gather_finish(buf, stage, r):
        for k in range(chips):
            theirs = block_of(buf, r, behind(k, pair))
            pair_copy(stage, r, k, theirs, theirs).wait_recv()

    def gather_sent(buf, stage, r):
        mine = block_of(buf, r, t)
        for k in range(1, chips):
            far_copy(stage, r, k, mine, mine, ahead(k)).wait_send()
        for k in range(chips):
            pair_copy(stage, r, k, mine, mine).wait_send()

    def to_pair(r, k):
        return pair_copy(1, r, k, block_of(part, r, ahead(k, pair)), pair_recv.at[r, k])

    def to_far(r, k):
        return far_copy(1, r, k, block_of(part, r, ahead(k)), far_recv.at[r, k], ahead(k))

    def sum_send(r):
        for k in range(chips - 1, -1, -1):
            to_pair(r, k).start()

    def sum_relay(r):
        for k in range(1, chips):
            to_pair(r, k).wait_recv()

            @pl.loop(0, rows // 64)
            def _(i):
                inside = pl.ds(pl.multiple_of(i * 64, 64), 64)
                at = pl.ds(pl.multiple_of(r * rows + i * 64, 64), 64)
                both = part[at, own_columns(ahead(k))].astype(F32) + pair_recv[r, k, inside, :].astype(F32)
                part[at, own_columns(ahead(k))] = both.astype(BF16)

            to_far(r, k).start()

    def summed(r, start, size):
        inside = pl.ds(pl.multiple_of(start, size), size)
        at = pl.ds(pl.multiple_of(r * rows + start, size), size)
        total = part[at, own_columns(t)].astype(F32) + pair_recv[r, 0, inside, :].astype(F32)
        for k in range(1, chips):
            total = total + far_recv[r, k, inside, :].astype(F32)
        return at, total

    def first_rows(r):
        to_pair(r, 0).wait_recv()
        for k in range(1, chips):
            to_far(r, k).wait_recv()

        @pl.loop(0, rows // 64)
        def _(i):
            at, total = summed(r, i * 64, 64)
            first_full[at, own_columns(t)] = (tok_full[at, own_columns(t)].astype(F32) + total).astype(BF16)

    def norm_rows(source, gain, r):
        size = 32

        @pl.loop(0, rows // size)
        def _(i):
            at = pl.ds(pl.multiple_of(r * rows + i * size, size), size)
            values = source[at, :].astype(F32)
            scale = lax.rsqrt(jnp.sum(values * values, axis=1, keepdims=True) / width + 1e-06)
            normed[at, :] = (values * scale * gain[...]).astype(BF16)

    channels = w0.shape[1]
    block = w3.shape[1]
    units = w4.shape[1]
    tap_count = taps_ref.shape[0]

    def mixer(r):
        for w in range(3):
            weight = full[w][...].reshape(width, channels)
            proj[w] = jnp.dot(normed[set_rows(r), :], weight, preferred_element_type=F32).astype(BF16)
        taps = taps_ref[:, pl.ds(pl.multiple_of(t * channels, 128), channels)]

        @pl.loop(0, seqs)
        def _(i):
            at = pl.ds(pl.multiple_of(i * length, length), length)
            product = proj[1, at, :].astype(F32) * proj[2, at, :].astype(F32)
            position = lax.broadcasted_iota(jnp.int32, product.shape, 0)
            conv = jnp.zeros_like(product)
            for offset in range(tap_count):
                shift = tap_count - 1 - offset
                moved = product if shift == 0 else jnp.where(position >= shift, pltpu.roll(product, shift, 0), 0.0)
                conv = conv + taps[offset : offset + 1, :] * moved
            gated[at, :] = (proj[0, at, :].astype(F32) * conv).astype(BF16)

        @pl.loop(0, n)
        def _(b):
            at = pl.ds(pl.multiple_of(b * block, 128), block)
            part[set_rows(r), at] = jnp.dot(gated[...], full[3][b], preferred_element_type=F32).astype(BF16)

    def hidden_tile(r, start, size):
        at = pl.ds(start, size)
        left = normed[set_rows(r), :]
        gate = jnp.dot(left, full[GATE][:, :, at].reshape(width, size), preferred_element_type=F32)
        upward = jnp.dot(left, full[UP][:, :, at].reshape(width, size), preferred_element_type=F32)
        hidden[set_rows(r), at] = (gate / (1.0 + jnp.exp(-gate)) * upward).astype(BF16)

    def hidden_rows(r):
        @pl.loop(0, units // 256)
        def _(j):
            hidden_tile(r, pl.multiple_of(j * 256, 256), 256)

        if units % 256:
            hidden_tile(r, units // 256 * 256, units % 256)

    wide = w6.shape[1]
    piece = min(wide, columns)
    per_block, per_owner = wide // piece, columns // piece

    def down_to_pair(r, k, slot, start):
        inside = pl.ds(pl.multiple_of(slot * piece, 128), piece)
        return pltpu.make_async_remote_copy(
            src_ref=part.at[set_rows(r), pl.ds(start, piece)], dst_ref=pair_recv.at[r, k, :, inside],
            send_sem=down_pair_ss.at[r, k, slot], recv_sem=down_pair_rs.at[r, k, slot],
            device_id={"tp": pair}, device_id_type=MESH,
        )

    def down_to_far(r, k, slot, start):
        inside = pl.ds(pl.multiple_of(slot * piece, 128), piece)
        return pltpu.make_async_remote_copy(
            src_ref=part.at[set_rows(r), pl.ds(start, piece)], dst_ref=far_recv.at[r, k, :, inside],
            send_sem=down_far_ss.at[r, k, slot], recv_sem=down_far_rs.at[r, k, slot],
            device_id={"tp": lax.rem(t + 2 * k, n_tp)}, device_id_type=MESH,
        )

    def down_block(b):
        for p in range(per_block):
            start = pl.multiple_of(b * wide + p * piece, 128)
            owner = (b * wide + p * piece) // columns
            slot = lax.rem(b * per_block + p, per_owner)
            k = lax.rem(owner // 2 - t // 2 + chips, chips)
            lane = lax.rem(owner, 2) == core

            @pl.loop(0, 2)
            def _(turn):
                r = 1 - turn
                at = pl.ds(pl.multiple_of(r * rows, rows), rows)
                weight = full[DOWN][b][:, p * piece : (p + 1) * piece]
                part[at, pl.ds(start, piece)] = jnp.dot(
                    hidden[at, :], weight, preferred_element_type=F32
                ).astype(BF16)

                @pl.when(jnp.logical_not(lane))
                def _():
                    down_to_pair(r, k, slot, start).start()

            @pl.when(lane & (k > 0))
            def _():
                for r in (1, 0):
                    down_to_pair(r, k, slot, start).wait_recv()
                    inside = pl.ds(pl.multiple_of(slot * piece, 128), piece)

                    @pl.loop(0, rows // 64)
                    def _(i):
                        here = pl.ds(pl.multiple_of(i * 64, 64), 64)
                        at = pl.ds(pl.multiple_of(r * rows + i * 64, 64), 64)
                        both = part[at, pl.ds(start, piece)].astype(F32) + pair_recv[r, k, here, inside].astype(F32)
                        part[at, pl.ds(start, piece)] = both.astype(BF16)

                    down_to_far(r, k, slot, start).start()

    def square_copy(r, k, peer):
        return pltpu.make_async_remote_copy(
            src_ref=sq_send.at[r], dst_ref=sq_recv.at[r, k - 1], send_sem=sq_ss.at[r, k - 1],
            recv_sem=sq_rs.at[r, k - 1], device_id={"tp": peer}, device_id_type=MESH,
        )

    def squares_send(r):
        for slot in range(per_owner):
            down_to_pair(r, 0, slot, 0).wait_recv()
            for k in range(1, chips):
                down_to_far(r, k, slot, 0).wait_recv()

        @pl.loop(0, seqs)
        def _(i):
            at, total = summed(r, i * length, length)
            second = first_full[at, own_columns(t)].astype(F32) + total
            squares = jnp.sum(second * second, axis=1, keepdims=True)
            sq_send[r, i] = jnp.transpose(jnp.broadcast_to(squares, (length, length)))[:8, :]

        for k in range(1, n_tp):
            square_copy(r, k, lax.rem(t + k, n_tp)).start()

    def close(r, dst):
        for k in range(1, n_tp):
            square_copy(r, k, lax.rem(t + n_tp - k, n_tp)).wait_recv()
        gain = out_gain[:, own_columns(t)]

        @pl.loop(0, seqs)
        def _(i):
            at, total = summed(r, i * length, length)
            second = first_full[at, own_columns(t)].astype(F32) + total
            squares = sq_send[r, i]
            for k in range(1, n_tp):
                squares = squares + sq_recv[r, k - 1, i]
            factor = column(lax.rsqrt(squares[:1, :] / width + 1e-06))
            inside = pl.ds(pl.multiple_of(i * length, length), length)
            dst[inside, :] = (second * factor * gain).astype(BF16)

    guest = lax.select(f == 1, 0, n - 1)
    has_guest = (f == 1) | (f == n - 2)
    inner = lax.select(f == 0, 1, n - 2)

    def tokens_in(device):
        return pltpu.make_async_remote_copy(
            src_ref=tok_ref, dst_ref=block_of(tok_full, 1, t), send_sem=guest_sem.at[0], recv_sem=guest_sem.at[1],
            device_id={"fs": device}, device_id_type=MESH,
        )

    def result_out(device):
        return pltpu.make_async_remote_copy(
            src_ref=returned, dst_ref=returned, send_sem=guest_sem.at[2], recv_sem=guest_sem.at[3],
            device_id={"fs": device}, device_id_type=MESH,
        )

    @pl.when(jnp.logical_not(is_host))
    def _():
        def halves(w, wait):
            @pl.loop(0, chunk_counts[w])
            def _(c):
                for k in range(1, parts):
                    if wait:
                        other_half(w, c, k).wait_send()
                    else:
                        other_half(w, c, k).start()

        tokens_in(inner).start()
        for w in range(MIXER):
            start_own(w)
        for w in range(MIXER):
            halves(w, False)
        for w in range(MIXER, 7):
            start_own(w)
            halves(w, False)
        tokens_in(inner).wait_send()
        for w in range(7):
            halves(w, True)

            @pl.loop(0, chunk_counts[w])
            def _(c):
                src = own[w].at[span(w, g, c), :]

                @pl.when(f == 0)
                def _():
                    z_copy(w, c, f, src, 1).wait_send()

                @pl.when(f == n - 1)
                def _():
                    z_copy(w, c, f, src, -1).wait_send()

        result_out(inner).wait_recv()
        out_ref[...] = returned[...]

    @pl.when(is_host)
    def _():
        own_tokens = pltpu.make_async_copy(tok_ref, block_of(tok_full, 0, t), own_sem.at[7])
        own_tokens.start()
        for w in range(MIXER):
            start_own(w)
        for w in range(7):
            own_copy(w).start()
        own_tokens.wait()
        gather_send(tok_full, 0, 0)
        steps = range(n - 2)
        for s in steps:
            receive(0, s)

        @pl.when(has_guest)
        def _():
            tokens_in(guest).wait_recv()

        gather_send(tok_full, 0, 1)
        gather_relay(tok_full, 0, 0)
        for w in range(1, MIXER):
            for s in steps:
                receive(w, s)
        start_own(GATE)
        gather_finish(tok_full, 0, 0)
        norm_rows(tok_full, mix_gain, 0)
        for w in range(MIXER):
            own_copy(w).wait()
            for s in steps:
                finish(w, s)
        mixer(0)
        sum_send(0)
        gather_relay(tok_full, 0, 1)
        receive(GATE, 0)
        start_own(UP)
        gather_finish(tok_full, 0, 1)
        norm_rows(tok_full, mix_gain, 1)
        sum_relay(0)
        mixer(1)
        sum_send(1)
        first_rows(0)
        gather_send(first_full, 2, 0)
        sum_relay(1)
        for s in steps[1:]:
            receive(GATE, s)
        receive(UP, 0)
        start_own(DOWN)
        gather_relay(first_full, 2, 0)
        first_rows(1)
        gather_send(first_full, 2, 1)
        gather_finish(first_full, 2, 0)
        norm_rows(first_full, ffn_gain, 0)
        for s in steps[1:]:
            receive(UP, s)
        gather_relay(first_full, 2, 1)
        for w in (GATE, UP):
            own_copy(w).wait()
            for s in steps:
                finish(w, s)
        hidden_rows(0)
        receive(DOWN, 0)
        gather_finish(first_full, 2, 1)
        norm_rows(first_full, ffn_gain, 1)
        hidden_rows(1)
        for r in range(2):
            for k in range(chips):
                to_pair(r, k).wait_send()
            for k in range(1, chips):
                to_far(r, k).wait_send()
        own_copy(DOWN).wait()
        down_block(f)

        for s in steps:
            if s > 0:
                receive(DOWN, s)
            finish(DOWN, s)

            @pl.loop(0, 2)
            def _(side):
                b = lax.select(side == 0, f - 1 - s, f + 1 + s)

                @pl.when((b >= 0) & (b < n))
                def _():
                    down_block(b)

        squares_send(1)
        squares_send(0)
        close(1, returned)

        @pl.when(has_guest)
        def _():
            result_out(guest).start()

        close(0, out_ref)

        @pl.when(has_guest)
        def _():
            result_out(guest).wait_send()

        for r in range(2):
            gather_sent(tok_full, 0, r)
            gather_sent(first_full, 2, r)
            for k in range(1, n_tp):
                square_copy(r, k, lax.rem(t + k, n_tp)).wait_send()
            for slot in range(per_owner):
                for k in range(chips):
                    down_to_pair(r, k, slot, 0).wait_send()
                for k in range(1, chips):
                    down_to_far(r, k, slot, 0).wait_send()
        for w in range(7):
            @pl.loop(0, chunk_counts[w])
            def _(c):
                @pl.loop(0, n)
                def _(blk):
                    here = region(w, blk, g, c)

                    @pl.when((f + 1 <= last_host) & (blk <= f))
                    def _():
                        z_copy(w, c, blk, here, 1).wait_send()

                    @pl.when((f - 1 >= first_host) & (blk >= f))
                    def _():
                        z_copy(w, c, blk, here, -1).wait_send()

                    whole = ((blk == 0) & (f == 1)) | ((blk == n - 1) & (f == n - 2))

                    @pl.when((blk != f) & jnp.logical_not(whole))
                    def _():
                        for k in range(1, parts):
                            y_copy(w, c, blk, g, k, y_peer(k)).wait_send()


def solution(mesh):
    n, parts, n_tp = mesh.shape["fs"], mesh.shape["grp"], mesh.shape["tp"]

    def local(tokens, mix_gain, outer, inner, value, taps, mix_out, ffn_gain, gate, up, down, out_gain):
        seqs, length, columns = tokens.shape
        rows, width = seqs * length, columns * n_tp
        weights = (outer, inner, value, mix_out, gate, up, down)
        counts = tuple(1 if w < MIXER else chunks_of(a.shape[0] // parts) for w, a in enumerate(weights))
        slots = sum(counts)
        channels, units = outer.shape[1], gate.shape[1]
        others, y_others = max(n_tp - 1, 1), max(parts - 1, 1)
        per_owner = columns // min(down.shape[1], columns)
        dma = pltpu.SemaphoreType.DMA
        scratch = [pltpu.VMEM((n,) + a.shape, BF16) for a in weights]
        chips = n_tp // 2
        scratch += [
            pltpu.VMEM((2 * rows, width), BF16),
            pltpu.VMEM((2 * rows, width), BF16),
            pltpu.VMEM((3, rows, channels), BF16),
            pltpu.VMEM((rows, channels), BF16),
            pltpu.VMEM((2 * rows, width), BF16),
            pltpu.VMEM((2, chips, rows, columns), BF16),
            pltpu.VMEM((2, chips, rows, columns), BF16),
            pltpu.VMEM((2 * rows, width), BF16),
            pltpu.VMEM((2 * rows, units), BF16),
            pltpu.VMEM((rows, columns), BF16),
            pltpu.VMEM((2, seqs, 8, length), F32),
            pltpu.VMEM((2, others, seqs, 8, length), F32),
            dma((slots, n)), dma((slots, n)), dma((slots, n)),
            dma((slots, n, y_others)), dma((slots, n, y_others)),
            dma((8,)), dma((3, 2, chips)), dma((3, 2, chips)), dma((3, 2, chips)), dma((3, 2, chips)),
            dma((2, chips, per_owner)), dma((2, chips, per_owner)),
            dma((2, chips, per_owner)), dma((2, chips, per_owner)),
            dma((2, others)), dma((2, others)), dma((4,)),
        ]
        out = pl.pallas_call(
            functools.partial(kernel, n, parts, n_tp, length, counts),
            out_shape=jax.ShapeDtypeStruct((rows, columns), BF16),
            in_specs=[pl.BlockSpec(memory_space=pltpu.VMEM)] * 12,
            out_specs=pl.BlockSpec(memory_space=pltpu.VMEM),
            scratch_shapes=scratch,
            compiler_params=pltpu.CompilerParams(
                collective_id=0, has_side_effects=True, vmem_limit_bytes=62 * 1024 * 1024
            ),
        )(
            tokens.reshape(rows, columns), mix_gain[None], outer, inner, value, taps, mix_out,
            ffn_gain[None], gate, up, down, out_gain[None],
        )
        return out.reshape(seqs, length, columns)

    in_specs = (
        P(("grp", "fs"), None, "tp"), P(), P("fs", "tp"), P("fs", "tp"), P("fs", "tp"), P(), P("tp", "fs"),
        P(), P("fs", "tp"), P("fs", "tp"), P("tp", "fs"), P(),
    )
    out_specs = P(("grp", "fs"), None, "tp")
    return jax.shard_map(local, mesh=mesh, in_specs=in_specs, out_specs=out_specs, check_vma=False)
```

time: 237 us -> 200 us (0.84)
  the two profiles are of different devices: /device:TPU:0 before, /device:TPU:16 now
where the time goes in v2:
time: 200 us
  Pallas kernels  198 us (99%)
    pallas_call x1, Pallas kernels, local(): pl.pallas_call(functools.partial(kernel, n, parts, n_tp, length, counts),...  198 us

profile of v2, /device:TPU:16, one launch (start us, length us, event | category | flops | bytes accessed | tf_op | source)
XLA Modules:
  0.0 200.2 jit_solution(16337063646021104136)
XLA Ops:
  0.0 198.4 %shard_map.118 = bf16[512,512]{1,0:T(8,128)(2,1)} custom-call(bf16[512,512]{1,0:T(8,128)(2,1)} %bitcast.6, f32[1,2048]{1,0:T(1,128)} %bitcast.7, bf16[512,256]{1,0:T(8,128)(2,1)} %w0.1, bf16[512,256]{1,0:T(8,128)(2,1)} %w1.1, bf16[512,256]{1,0:T(8,128)(2,1)} %w2.1, f32[3,1024]{1,0:T(4,128)} %taps_ref.1, bf16[256,512]{1,0:T(8,128)(2,1)} %w3.1, ...), custom_call_target="tpu_custom_call" | custom-call | tf_op jit(solution)/shard_map/pallas_call | solution.py:622
  198.4 1.9 copy.14

commit v3 on v2

--- a/solution.py
+++ b/solution.py
@@ -12,6 +12,7 @@
 BF16 = jnp.bfloat16
 MIXER = 4
 GATE, UP, DOWN = 4, 5, 6
+SHARED = 2
 
 
 def chunks_of(half):
@@ -53,7 +54,22 @@
         return pl.ds(pl.multiple_of(start, 8), piece)
 
     def region(w, blk, half, c):
+        if w == DOWN:
+            return full[w].at[blk, half_rows(half), strip(c)]
         return full[w].at[blk, span(w, half, c), :]
+
+    def half_rows(half):
+        size = w6.shape[0] // parts
+        return pl.ds(pl.multiple_of(half * size, 8), size)
+
+    def strip(c):
+        size = w6.shape[1] // chunk_counts[DOWN]
+        return pl.ds(pl.multiple_of(c * size, 128), size)
+
+    def own_region(w, half, c):
+        if w == DOWN:
+            return own[w].at[half_rows(half), strip(c)]
+        return own[w].at[span(w, half, c), :]
 
     barrier = pltpu.get_barrier_semaphore()
     for k in range(1, n_tp):
@@ -93,30 +109,36 @@
     def start_own(w):
         @pl.loop(0, chunk_counts[w])
         def _(c):
-            src = own[w].at[span(w, g, c), :]
-
-            @pl.when(f + 1 <= last_host)
-            def _():
-                z_copy(w, c, f, src, 1).start()
-
-            @pl.when(f - 1 >= first_host)
-            def _():
-                z_copy(w, c, f, src, -1).start()
+            start_chunk(w, c)
+
+    def start_chunk(w, c):
+        src = own_region(w, g, c)
+
+        @pl.when(f + 1 <= last_host)
+        def _():
+            z_copy(w, c, f, src, 1).start()
+
+        @pl.when(f - 1 >= first_host)
+        def _():
+            z_copy(w, c, f, src, -1).start()
 
     def other_half(w, c, k):
         half = lax.rem(g + parts - k, parts)
         inward = lax.select(f == 0, 1, n - 2)
         return pltpu.make_async_remote_copy(
-            src_ref=own[w].at[span(w, half, c), :], dst_ref=region(w, f, half, c),
+            src_ref=own_region(w, half, c), dst_ref=region(w, f, half, c),
             send_sem=y_send.at[bases[w] + c, f, k - 1], recv_sem=y_recv.at[bases[w] + c, f, k - 1],
             device_id={"fs": inward}, device_id_type=MESH,
         )
 
     def receive(w, s):
-        left, right = f - 1 - s, f + 1 + s
-
         @pl.loop(0, chunk_counts[w])
         def _(c):
+            receive_chunk(w, s, c)
+
+    def receive_chunk(w, s, c):
+        left, right = f - 1 - s, f + 1 + s
+        if True:
             def arrived(blk, step, whole):
                 z_copy(w, c, blk, region(w, blk, g, c), -step).wait_recv()
                 onward = (f + 1 <= last_host) if step > 0 else (f - 1 >= first_host)
@@ -129,7 +151,7 @@
                     for k in range(1, parts):
                         y_copy(w, c, blk, g, k, y_peer(k)).start()
 
-                if s == 0:
+                if s == 0 and w >= SHARED:
                     pl.when(jnp.logical_not(whole))(share)
                 else:
                     share()
@@ -145,6 +167,10 @@
     def finish(w, s):
         @pl.loop(0, chunk_counts[w])
         def _(c):
+            finish_chunk(w, s, c)
+
+    def finish_chunk(w, s, c):
+        if True:
             for k in range(1, parts):
                 source = lax.rem(g + parts - k, parts)
                 for blk, there in ((f - 1 - s, f - 1 - s >= 0), (f + 1 + s, f + 1 + s < n)):
@@ -305,8 +331,8 @@
             hidden_tile(r, units // 256 * 256, units % 256)
 
     wide = w6.shape[1]
-    piece = min(wide, columns)
-    per_block, per_owner = wide // piece, columns // piece
+    piece = wide // chunk_counts[DOWN]
+    per_owner = columns // piece
 
     def down_to_pair(r, k, slot, start):
         inside = pl.ds(pl.multiple_of(slot * piece, 128), piece)
@@ -324,41 +350,46 @@
             device_id={"tp": lax.rem(t + 2 * k, n_tp)}, device_id_type=MESH,
         )
 
-    def down_block(b):
-        for p in range(per_block):
-            start = pl.multiple_of(b * wide + p * piece, 128)
-            owner = (b * wide + p * piece) // columns
-            slot = lax.rem(b * per_block + p, per_owner)
-            k = lax.rem(owner // 2 - t // 2 + chips, chips)
-            lane = lax.rem(owner, 2) == core
-
-            @pl.loop(0, 2)
-            def _(turn):
-                r = 1 - turn
-                at = pl.ds(pl.multiple_of(r * rows, rows), rows)
-                weight = full[DOWN][b][:, p * piece : (p + 1) * piece]
-                part[at, pl.ds(start, piece)] = jnp.dot(
-                    hidden[at, :], weight, preferred_element_type=F32
-                ).astype(BF16)
-
-                @pl.when(jnp.logical_not(lane))
+    def down_strip(c):
+        @pl.loop(0, 3)
+        def _(phase):
+            @pl.loop(0, n)
+            def _(b):
+                start = pl.multiple_of(b * wide + c * piece, 128)
+                owner = (b * wide + c * piece) // columns
+                slot = lax.rem((b * wide + c * piece) // piece, per_owner)
+                k = lax.rem(owner // 2 - t // 2 + chips, chips)
+                other = lax.rem(owner + t, 2)
+                mine = (1 - other) * (2 - lax.min(k, 1))
+
+                @pl.when(mine == phase)
                 def _():
-                    down_to_pair(r, k, slot, start).start()
-
-            @pl.when(lane & (k > 0))
-            def _():
-                for r in (1, 0):
-                    down_to_pair(r, k, slot, start).wait_recv()
-                    inside = pl.ds(pl.multiple_of(slot * piece, 128), piece)
-
-                    @pl.loop(0, rows // 64)
-                    def _(i):
-                        here = pl.ds(pl.multiple_of(i * 64, 64), 64)
-                        at = pl.ds(pl.multiple_of(r * rows + i * 64, 64), 64)
-                        both = part[at, pl.ds(start, piece)].astype(F32) + pair_recv[r, k, here, inside].astype(F32)
-                        part[at, pl.ds(start, piece)] = both.astype(BF16)
-
-                    down_to_far(r, k, slot, start).start()
+                    down_piece(b, c, start, slot, k, other)
+
+    def down_piece(b, c, start, slot, k, other):
+        part[:, pl.ds(start, piece)] = jnp.dot(
+            hidden[...], full[DOWN][b, :, strip(c)], preferred_element_type=F32
+        ).astype(BF16)
+
+        @pl.when(other == 1)
+        def _():
+            for r in (1, 0):
+                down_to_pair(r, k, slot, start).start()
+
+        @pl.when((other == 0) & (k > 0))
+        def _():
+            for r in (1, 0):
+                down_to_pair(r, k, slot, start).wait_recv()
+                inside = pl.ds(pl.multiple_of(slot * piece, 128), piece)
+
+                @pl.loop(0, rows // 64)
+                def _(i):
+                    here = pl.ds(pl.multiple_of(i * 64, 64), 64)
+                    at = pl.ds(pl.multiple_of(r * rows + i * 64, 64), 64)
+                    both = part[at, pl.ds(start, piece)].astype(F32) + pair_recv[r, k, here, inside].astype(F32)
+                    part[at, pl.ds(start, piece)] = both.astype(BF16)
+
+                down_to_far(r, k, slot, start).start()
 
     def square_copy(r, k, peer):
         return pltpu.make_async_remote_copy(
@@ -428,18 +459,26 @@
         tokens_in(inner).start()
         for w in range(MIXER):
             start_own(w)
-        for w in range(MIXER):
+        for w in range(SHARED, MIXER):
             halves(w, False)
-        for w in range(MIXER, 7):
+        for w in (GATE, UP):
             start_own(w)
             halves(w, False)
+
+        @pl.loop(0, chunk_counts[DOWN])
+        def _(c):
+            start_chunk(DOWN, c)
+            for k in range(1, parts):
+                other_half(DOWN, c, k).start()
+
         tokens_in(inner).wait_send()
         for w in range(7):
-            halves(w, True)
+            if w >= SHARED:
+                halves(w, True)
 
             @pl.loop(0, chunk_counts[w])
             def _(c):
-                src = own[w].at[span(w, g, c), :]
+                src = own_region(w, g, c)
 
                 @pl.when(f == 0)
                 def _():
@@ -512,7 +551,8 @@
             for s in steps:
                 finish(w, s)
         hidden_rows(0)
-        receive(DOWN, 0)
+        for s in steps:
+            receive_chunk(DOWN, s, 0)
         gather_finish(first_full, 2, 1)
         norm_rows(first_full, ffn_gain, 1)
         hidden_rows(1)
@@ -522,20 +562,17 @@
             for k in range(1, chips):
                 to_far(r, k).wait_send()
         own_copy(DOWN).wait()
-        down_block(f)
-
-        for s in steps:
-            if s > 0:
-                receive(DOWN, s)
-            finish(DOWN, s)
-
-            @pl.loop(0, 2)
-            def _(side):
-                b = lax.select(side == 0, f - 1 - s, f + 1 + s)
-
-                @pl.when((b >= 0) & (b < n))
-                def _():
-                    down_block(b)
+
+        @pl.loop(0, chunk_counts[DOWN])
+        def _(c):
+            @pl.when(c > 0)
+            def _():
+                for s in steps:
+                    receive_chunk(DOWN, s, c)
+
+            for s in steps:
+                finish_chunk(DOWN, s, c)
+            down_strip(c)
 
         squares_send(1)
         squares_send(0)
@@ -577,6 +614,8 @@
                         z_copy(w, c, blk, here, -1).wait_send()
 
                     whole = ((blk == 0) & (f == 1)) | ((blk == n - 1) & (f == n - 2))
+                    if w < SHARED:
+                        whole = blk == f
 
                     @pl.when((blk != f) & jnp.logical_not(whole))
                     def _():
@@ -592,10 +631,13 @@
         rows, width = seqs * length, columns * n_tp
         weights = (outer, inner, value, mix_out, gate, up, down)
         counts = tuple(1 if w < MIXER else chunks_of(a.shape[0] // parts) for w, a in enumerate(weights))
+        wide = down.shape[1]
+        strips = next(count for count in (4, 2, 1) if wide % (count * 128) == 0 or count == 1)
+        counts = counts[:-1] + (strips,)
         slots = sum(counts)
         channels, units = outer.shape[1], gate.shape[1]
         others, y_others = max(n_tp - 1, 1), max(parts - 1, 1)
-        per_owner = columns // min(down.shape[1], columns)
+        per_owner = columns * strips // wide
         dma = pltpu.SemaphoreType.DMA
         scratch = [pltpu.VMEM((n,) + a.shape, BF16) for a in weights]
         chips = n_tp // 2

time: 200 us -> 225 us (1.12)
  Pallas kernels: 198 us -> 222 us
    pallas_call x1, Pallas kernels: 198 us -> 222 us  [local(): pl.pallas_call(functools.partial(kernel, n, parts, n_tp, length, counts),...]
where the time goes in v3:
time: 225 us; the launch traced here: 223 us
  Pallas kernels  222 us (99%)
    pallas_call x1, Pallas kernels, local(): pl.pallas_call(functools.partial(kernel, n, parts, n_tp, length, counts),...  222 us

profile of v3, /device:TPU:16, one launch (start us, length us, event | category | flops | bytes accessed | tf_op | source)
XLA Modules:
  0.0 223.5 jit_solution(1348794362255856927)
XLA Ops:
  0.0 221.6 %shard_map.118 = bf16[512,512]{1,0:T(8,128)(2,1)} custom-call(bf16[512,512]{1,0:T(8,128)(2,1)} %bitcast.6, f32[1,2048]{1,0:T(1,128)} %bitcast.7, bf16[512,256]{1,0:T(8,128)(2,1)} %w0.1, bf16[512,256]{1,0:T(8,128)(2,1)} %w1.1, bf16[512,256]{1,0:T(8,128)(2,1)} %w2.1, f32[3,1024]{1,0:T(4,128)} %taps_ref.1, bf16[256,512]{1,0:T(8,128)(2,1)} %w3.1, ...), custom_call_target="tpu_custom_call" | custom-call | tf_op jit(solution)/shard_map/pallas_call | solution.py:664
  221.6 1.9 copy.14

commit v4 on v2

--- a/solution.py
+++ b/solution.py
@@ -12,6 +12,7 @@
 BF16 = jnp.bfloat16
 MIXER = 4
 GATE, UP, DOWN = 4, 5, 6
+SHARED = 2
 
 
 def chunks_of(half):
@@ -129,7 +130,7 @@
                     for k in range(1, parts):
                         y_copy(w, c, blk, g, k, y_peer(k)).start()
 
-                if s == 0:
+                if s == 0 and w >= SHARED:
                     pl.when(jnp.logical_not(whole))(share)
                 else:
                     share()
@@ -428,14 +429,15 @@
         tokens_in(inner).start()
         for w in range(MIXER):
             start_own(w)
-        for w in range(MIXER):
+        for w in range(SHARED, MIXER):
             halves(w, False)
         for w in range(MIXER, 7):
             start_own(w)
             halves(w, False)
         tokens_in(inner).wait_send()
         for w in range(7):
-            halves(w, True)
+            if w >= SHARED:
+                halves(w, True)
 
             @pl.loop(0, chunk_counts[w])
             def _(c):
@@ -577,6 +579,8 @@
                         z_copy(w, c, blk, here, -1).wait_send()
 
                     whole = ((blk == 0) & (f == 1)) | ((blk == n - 1) & (f == n - 2))
+                    if w < SHARED:
+                        whole = blk == f
 
                     @pl.when((blk != f) & jnp.logical_not(whole))
                     def _():

time: 200 us -> 205 us (1.025); the launches traced: 200 us -> 203 us
  Pallas kernels: 198 us -> 201 us
    pallas_call x1, Pallas kernels: 198 us -> 201 us  [local(): pl.pallas_call(functools.partial(kernel, n, parts, n_tp, length, counts),...]
where the time goes in v4:
time: 205 us; the launch traced here: 203 us
  Pallas kernels  201 us (98%)
    pallas_call x1, Pallas kernels, local(): pl.pallas_call(functools.partial(kernel, n, parts, n_tp, length, counts),...  201 us

profile of v4, /device:TPU:16, one launch (start us, length us, event | category | flops | bytes accessed | tf_op | source)
XLA Modules:
  0.0 203.1 jit_solution(12983972064934966474)
XLA Ops:
  0.0 201.2 %shard_map.118 = bf16[512,512]{1,0:T(8,128)(2,1)} custom-call(bf16[512,512]{1,0:T(8,128)(2,1)} %bitcast.6, f32[1,2048]{1,0:T(1,128)} %bitcast.7, bf16[512,256]{1,0:T(8,128)(2,1)} %w0.1, bf16[512,256]{1,0:T(8,128)(2,1)} %w1.1, bf16[512,256]{1,0:T(8,128)(2,1)} %w2.1, f32[3,1024]{1,0:T(4,128)} %taps_ref.1, bf16[256,512]{1,0:T(8,128)(2,1)} %w3.1, ...), custom_call_target="tpu_custom_call" | custom-call | tf_op jit(solution)/shard_map/pallas_call | solution.py:626
  201.2 1.9 copy.14
